TPU v7x, 32 devices: a whole 2x2x4 slice. The times are simulated.
32 devices in a mesh: gr: 2 (over core), fs: 8 (over z, y), tp: 2 (over x).
Axes of the slice: x: 2, y: 2, z: 4, core: 2. Of those that a mesh axis runs over, the one named last changes fastest.
Arguments:
- prompt: bfloat16 [5120, 2048], P(('gr', 'fs'), 'tp'), may hold values from -6 to 6
- norm_gain: float32 [2048], P(('gr', 'fs')), may hold values from 0.1 to 1.9
- gate_weight: float32 [32, 2048, 2048], P(None, ('gr', 'fs'), 'tp'), may hold values from -0.125 to 0.125
- up_weight: float32 [32, 2048, 2048], P(None, ('gr', 'fs'), 'tp'), may hold values from -0.125 to 0.125
- down_weight: float32 [32, 2048, 2048], P(None, ('gr', 'fs'), 'tp'), may hold values from -0.125 to 0.125
- routes: int32 [5120, 2], P(('gr', 'fs')), may hold values from 0 to 31, as said below
- route_weight: float32 [5120, 2], P(('gr', 'fs')), may hold values from 0.2 to 1
Outputs:
- gate_new: bfloat16 [32, 2048, 2048], P('fs', None, 'tp')
- up_new: bfloat16 [32, 2048, 2048], P('fs', None, 'tp')
- down_new: bfloat16 [32, 2048, 2048], P('fs', 'tp')
- mixed: bfloat16 [5120, 2048], P(('gr', 'fs'), 'tp')
Inputs may be any that keep to these rules, and one draw needn't show every extreme that they name: `routes`: each row names two different experts of the same group; expert e belongs to group e // 8. Among the 320 rows of one index of gr and fs no expert is named more than 30 times, and in every draw every expert of one group is named exactly 30 times by the rows of every index.
All inputs are finite; a program needn't handle non-finite values.
Results may differ from a plain program's by a relative error of at most 0.015.
Values may be sent and summed in bfloat16 or wider, within the bound.
A program may use at most 256 MiB of HBM per device.

v0:
```python
import jax
import jax.numpy as jnp
from jax import lax
from jax.sharding import PartitionSpec as P

CAP = 30


def body(prompt, norm_gain, gate_weight, up_weight, down_weight, routes, route_weight):
    groups_fs = lax.axis_size("fs")
    groups_tp = lax.axis_size("tp")
    gate_cast = (gate_weight * norm_gain[None, :, None]).astype(jnp.bfloat16)
    up_cast = (up_weight * norm_gain[None, :, None]).astype(jnp.bfloat16)
    down_cast = down_weight.astype(jnp.bfloat16)
    spread = (
        lax.all_to_all(gate_cast, "fs", split_axis=0, concat_axis=1, tiled=True),
        lax.all_to_all(up_cast, "fs", split_axis=0, concat_axis=1, tiled=True),
        lax.all_to_all(down_cast, "fs", split_axis=0, concat_axis=1, tiled=True),
    )
    gate_new, up_new, down_rows = (
        lax.all_gather(spread[0], "gr", axis=1, tiled=True),
        lax.all_gather(spread[1], "gr", axis=1, tiled=True),
        lax.all_gather(spread[2], "gr", axis=1, tiled=True),
    )
    down_new = lax.all_to_all(down_rows, "tp", split_axis=1, concat_axis=2, tiled=True)
    values = prompt.astype(jnp.float32)
    tok_count = prompt.shape[0]
    col_width = prompt.shape[1]
    full_width = col_width * groups_tp
    squares = jnp.sum(values * values, axis=-1, keepdims=True)
    total_squares = lax.psum(squares, "tp")
    normed = (values * lax.rsqrt(total_squares / full_width + 1e-06)).astype(jnp.bfloat16)
    expert_total = gate_weight.shape[0]
    per_device = expert_total // groups_fs
    slots_all = expert_total * CAP
    picks_flat = routes.reshape(-1)
    matches = (picks_flat[:, None] == jnp.arange(expert_total, dtype=jnp.int32)[None, :]).astype(
        jnp.int32
    )
    earlier = jnp.cumsum(matches, axis=0) - matches
    slot_of = jnp.sum(earlier * matches, axis=1)
    target = (picks_flat * CAP + slot_of).reshape(tok_count, 2)
    slot_ids = jnp.arange(slots_all, dtype=jnp.int32)[None, :]
    select_first = (target[:, 0:1] == slot_ids).astype(jnp.bfloat16)
    select_second = (target[:, 1:2] == slot_ids).astype(jnp.bfloat16)
    select_both = select_first + select_second
    outbound = jnp.einsum("ts,td->sd", select_both, normed, preferred_element_type=jnp.float32)
    outbound = outbound.astype(jnp.bfloat16).reshape(groups_fs, per_device, CAP, col_width)
    full_rows = lax.all_gather(outbound, "tp", axis=3, tiled=True)
    arrived = lax.all_to_all(full_rows, "fs", split_axis=0, concat_axis=0, tiled=True)
    gate_pre = jnp.einsum("sxcd,xdh->sxch", arrived, gate_new, preferred_element_type=jnp.float32)
    up_pre = jnp.einsum("sxcd,xdh->sxch", arrived, up_new, preferred_element_type=jnp.float32)
    hidden = (jax.nn.silu(gate_pre) * up_pre).astype(jnp.bfloat16)
    partial_value = jnp.einsum(
        "sxch,xhd->sxcd", hidden, down_new, preferred_element_type=jnp.float32
    )
    summed = lax.psum_scatter(
        partial_value.astype(jnp.bfloat16), "tp", scatter_dimension=3, tiled=True
    )
    returned = lax.all_to_all(summed, "fs", split_axis=0, concat_axis=0, tiled=True)
    returned_flat = returned.reshape(slots_all, returned.shape[3])
    pick_first = jnp.dot(select_first, returned_flat, preferred_element_type=jnp.float32)
    pick_second = jnp.dot(select_second, returned_flat, preferred_element_type=jnp.float32)
    mixed = route_weight[:, 0:1] * pick_first + route_weight[:, 1:2] * pick_second
    return (gate_new, up_new, down_new, mixed.astype(jnp.bfloat16))


def solution(mesh):
    return jax.shard_map(
        body,
        mesh=mesh,
        in_specs=(
            P(("gr", "fs"), "tp"),
            P(("gr", "fs")),
            P(None, ("gr", "fs"), "tp"),
            P(None, ("gr", "fs"), "tp"),
            P(None, ("gr", "fs"), "tp"),
            P(("gr", "fs"), None),
            P(("gr", "fs"), None),
        ),
        out_specs=(
            P("fs", None, "tp"),
            P("fs", None, "tp"),
            P("fs", "tp", None),
            P(("gr", "fs"), "tp"),
        ),
        check_vma=False,
    )
```

profile of v0, /device:TPU:0, one launch (start us, length us, event | category | flops | bytes accessed | tf_op | source)
XLA Modules:
  0.0 1178.5 jit_solution(15978841417502399266)
XLA Ops:
  7.2 9.1 convert_element_type.45
  16.2 7.4 all-to-all-start.2
  26.5 4.9 psum.7
  35.2 171.6 %all-to-all-done.2 = bf16[32,128,1024]{2,1,0:T(8,128)(2,1)} async-done(((bf16[32,128,1024]{2,1,0:T(8,128)(2,1)}), bf16[32,128,1024]{2,1,0:T(8,128)(2,1)}, u32[]{:S(2)}, u32[]{:S(2)}) %all-to-all-start.2) | async-done | bytes 8388640 | tf_op jit(solution)/shard_map/all_to_all | solution.py:18
  206.9 8.2 copy.53
  215.7 20.4 %multiply_convert_fusion = (bf16[32,128,1024]{2,1,0:T(8,128)(2,1)S(1)}, bf16[32,128,1024]{2,1,0:T(8,128)(2,1)}) fusion(f32[32,128,1024]{2,1,0:T(8,128)} %param.10, f32[128]{0:T(128)S(1)} %copy-done.9, f32[32,128,1024]{2,1,0:T(8,128)} %param.9), kind=kLoop, calls=%fused_computation.6 | loop fusion | flops 16777216 | bytes 50332160 | tf_op jit(solution)/shard_map/convert_element_type | solution.py:13
  236.1 186.2 %all_to_all.82 = bf16[32,128,1024]{2,1,0:T(8,128)(2,1)} all-to-all(bf16[32,128,1024]{2,1,0:T(8,128)(2,1)S(1)} %get-tuple-element.8), channel_id=1, replica_groups=mesh['gr'=2,'fs'=8,'tp'=2] {'fs'}, dimensions={0} | all-to-all | bytes 16777216 | tf_op jit(solution)/shard_map/all_to_all | solution.py:17
  422.3 8.4 copy.52
  430.8 187.6 %all_to_all.83 = bf16[32,128,1024]{2,1,0:T(8,128)(2,1)} all-to-all(bf16[32,128,1024]{2,1,0:T(8,128)(2,1)} %get-tuple-element.9), channel_id=1, replica_groups=mesh['gr'=2,'fs'=8,'tp'=2] {'fs'}, dimensions={0} | all-to-all | bytes 16777216 | tf_op jit(solution)/shard_map/all_to_all | solution.py:16
  618.4 8.4 copy.51
  626.8 7.7 copy.61
  634.5 4.9 all-to-all-start.4
  639.5 22.3 %copy.54 = bf16[4,2048,1024]{2,0,1:T(4,128)(2,1)} copy(bf16[4,2048,1024]{2,1,0:T(8,128)(2,1)} %all-gather.9.cloned.1.call-done) | data formatting | bytes 33554432 | tf_op jit(solution)/shard_map/all_gather | solution.py:23
  661.8 63.6 %all-to-all-done.4 = bf16[8,4,30,2048]{3,1,2,0:T(4,128)(2,1)} async-done(((bf16[8,4,30,2048]{3,1,2,0:T(4,128)(2,1)}), bf16[8,4,30,2048]{3,1,2,0:T(4,128)(2,1)}, u32[]{:S(2)}, u32[]{:S(2)}) %all-to-all-start.4) | async-done | bytes 3932192 | tf_op jit(solution)/shard_map/all_to_all | solution.py:50
  725.4 9.7 all-to-all-start.3
  735.1 15.3 %fusion = f32[4,1024,8,30]{1,3,2,0:T(8,128)} fusion(bf16[4,2048,1024]{2,1,0:T(8,128)(2,1)} %all-gather.7.cloned.1.call-done, bf16[8,4,30,2048]{3,1,2,0:T(4,128)(2,1)} %all-to-all-done.4), kind=kOutput, calls=%fused_computation | convolution fusion | flops 4026531840 | bytes 24641536 | tf_op jit(solution)/shard_map/sxcd,xdh->sxch/dot_general | solution.py:52
  750.5 14.9 %fusion.6 = bf16[8,4,30,1024]{3,2,0,1:T(8,128)(2,1)S(1)} fusion(f32[4,1024,8,30]{1,3,2,0:T(8,128)} %fusion, bf16[8,4,30,2048]{3,1,2,0:T(4,128)(2,1)} %all-to-all-done.4, bf16[4,2048,1024]{2,1,0:T(8,128)(2,1)} %all-gather.5.cloned.1.call-done), kind=kOutput, calls=%fused_computation.9 | convolution fusion | flops 4032430080 | bytes 26607616 | tf_op jit(solution)/shard_map/sxcd,xdh->sxch/dot_general | solution.py:51
  765.4 150.2 %all-to-all-done.3 = bf16[4,2048,1024]{2,0,1:T(4,128)(2,1)} async-done(((bf16[4,2048,1024]{2,0,1:T(4,128)(2,1)}), bf16[4,2048,1024]{2,0,1:T(4,128)(2,1)}, u32[]{:S(2)}, u32[]{:S(2)}) %all-to-all-start.3) | async-done | bytes 16777248 | tf_op jit(solution)/shard_map/all_to_all | solution.py:25
  915.5 12.3 %copy.55 = bf16[4,2048,1024]{2,1,0:T(8,128)(2,1)S(1)} copy(bf16[4,2048,1024]{2,0,1:T(4,128)(2,1)} %all-to-all-done.3) | data formatting | bytes 33554432 | tf_op jit(solution)/shard_map/all_to_all | solution.py:25
  927.9 6.2 copy-done
  934.0 57.6 %copy.56 = bf16[4,1024,2,1024]{3,2,1,0:T(2,128)(2,1)} copy(bf16[4,1024,2,1024]{3,1,2,0:T(8,128)(2,1)S(1)} %bitcast.76) | data formatting | bytes 33554432 | tf_op jit(solution)/shard_map/all_to_all | solution.py:25
  991.6 27.7 %reshape.40 = bf16[4,1024,2048,1]{2,1,0,3:T(8,128)(2,1)} reshape(bf16[4,1024,2,1024]{3,2,1,0:T(2,128)(2,1)} %copy.56) | data formatting | bytes 33554432 | tf_op jit(solution)/shard_map/all_to_all | solution.py:25
  1019.3 11.8 %convert_bitcast_fusion = bf16[8,4,30,2048]{3,2,0,1:T(8,128)(2,1)} fusion(bf16[8,4,30,1024]{3,2,0,1:T(8,128)(2,1)S(1)} %fusion.6, bf16[4,1024,2048,1]{2,1,0,3:T(8,128)(2,1)} %reshape.40), kind=kOutput, calls=%fused_computation.15 | convolution fusion | flops 4028497920 | bytes 22675456 | tf_op jit(solution)/shard_map/sxch,xhd->sxcd/dot_general | solution.py:54
  1031.1 55.2 %reduce-scatter.2.cloned.1.call-done = bf16[8,4,30,1024]{3,2,0,1:T(8,128)(2,1)} async-done(((bf16[8,4,30,2048]{3,2,0,1:T(8,128)(2,1)}), bf16[8,4,30,1024]{3,2,0,1:T(8,128)(2,1)}) %reduce-scatter.2.cloned.1.call-update) | async-done | bytes 1966096 | tf_op jit(solution)/shard_map/reduce_scatter | solution.py:57
  1086.3 4.4 copy.64
  1090.7 5.5 all-to-all-start.5
  1096.3 14.2 %copy.69 = bf16[4,2,128,8,1024]{4,3,1,2,0:T(8,128)(2,1)} copy(bf16[4,2,128,8,1024]{4,3,2,1,0:T(8,128)(2,1)} %bitcast.77) | data formatting | bytes 33554432 | tf_op jit(solution)/shard_map/all_to_all | solution.py:25
  1110.4 31.2 %all-to-all-done.5 = bf16[8,4,30,1024]{3,1,2,0:T(4,128)(2,1)} async-done(((bf16[8,4,30,1024]{3,1,2,0:T(4,128)(2,1)}), bf16[8,4,30,1024]{3,1,2,0:T(4,128)(2,1)}, u32[]{:S(2)}, u32[]{:S(2)}) %all-to-all-start.5) | async-done | bytes 1966112 | tf_op jit(solution)/shard_map/all_to_all | solution.py:60
  1141.6 2.2 copy.65
  1145.4 2.6 convolution_multiply_fusion.1
  1149.8 16.0 %copy.80 = bf16[4,2048,1024]{2,1,0:T(8,128)(2,1)} copy(bf16[4,2048,1024]{2,1,0:T(8,128)(2,1)} %all-gather.5.cloned.1.call-done) | data formatting | bytes 33554432
  1165.8 6.2 copy.81
  (62 shorter events, 10.7 us)
Async XLA Ops:
  16.2 7.5 copy-start.3
  16.2 7.9 copy-start.2
  16.2 190.6 %all-to-all-start.2 = ((bf16[32,128,1024]{2,1,0:T(8,128)(2,1)}), bf16[32,128,1024]{2,1,0:T(8,128)(2,1)}, u32[]{:S(2)}, u32[]{:S(2)}) async-start(bf16[32,128,1024]{2,1,0:T(8,128)(2,1)} %convert_element_type.45), calls=%async_computation.2 | async-start | bytes 16777216 | tf_op jit(solution)/shard_map/all_to_all | solution.py:18
  23.7 603.1 %all-gather.11.cloned.1.call-start = ((), (), s32[]{:S(2)}) async-start(), calls=%async_computation.10 | async-start | bytes 6291456 | tf_op jit(solution)/shard_map/all_gather | solution.py:49
  31.5 0.6 copy-start.5
  31.5 0.6 copy-start.7
  35.2 604.3 %all-gather.9.cloned.1.call-start = ((), (), s32[]{:S(2)}) async-start(), calls=%async_computation.9 | async-start | bytes 25165824 | tf_op jit(solution)/shard_map/all_gather | solution.py:23
  215.0 0.7 copy-start.9
  215.1 520.1 %all-gather.7.cloned.1.call-start = ((), (), s32[]{:S(2)}) async-start(), calls=%async_computation.8 | async-start | bytes 25165824 | tf_op jit(solution)/shard_map/all_gather | solution.py:22
  430.7 319.7 %all-gather.5.cloned.1.call-start = ((), (), s32[]{:S(2)}) async-start(), calls=%async_computation.7 | async-start | bytes 25165824 | tf_op jit(solution)/shard_map/all_gather | solution.py:21
  634.5 90.8 %all-to-all-start.4 = ((bf16[8,4,30,2048]{3,1,2,0:T(4,128)(2,1)}), bf16[8,4,30,2048]{3,1,2,0:T(4,128)(2,1)}, u32[]{:S(2)}, u32[]{:S(2)}) async-start(bf16[8,4,30,2048]{3,1,2,0:T(4,128)(2,1)} %copy.61), calls=%async_computation.4 | async-start | bytes 7864320 | tf_op jit(solution)/shard_map/all_to_all | solution.py:50
  725.4 190.2 %all-to-all-start.3 = ((bf16[4,2048,1024]{2,0,1:T(4,128)(2,1)}), bf16[4,2048,1024]{2,0,1:T(4,128)(2,1)}, u32[]{:S(2)}, u32[]{:S(2)}) async-start(bf16[4,2048,1024]{2,0,1:T(4,128)(2,1)} %copy.54), calls=%async_computation.3 | async-start | bytes 33554432 | tf_op jit(solution)/shard_map/all_to_all | solution.py:25
  735.1 351.3 %reduce-scatter.2.cloned.1.call-start = ((), (), s32[]{:S(2)}) async-start(), calls=%async_computation.11 | async-start | bytes 6291456 | tf_op jit(solution)/shard_map/reduce_scatter | solution.py:57
  927.9 6.2 copy-start
  1031.1 65.1 %copy-start.4 = (f32[320,2]{0,1:T(2,128)S(1)}, f32[320,2]{0,1:T(2,128)}, u32[]{:S(2)}) copy-start(f32[320,2]{0,1:T(2,128)} %param.13) | copy-start | bytes 7684
  1090.7 50.9 %all-to-all-start.5 = ((bf16[8,4,30,1024]{3,1,2,0:T(4,128)(2,1)}), bf16[8,4,30,1024]{3,1,2,0:T(4,128)(2,1)}, u32[]{:S(2)}, u32[]{:S(2)}) async-start(bf16[8,4,30,1024]{3,1,2,0:T(4,128)(2,1)} %copy.64), calls=%async_computation.6 | async-start | bytes 3932160 | tf_op jit(solution)/shard_map/all_to_all | solution.py:60
  1110.4 34.9 %copy-start.8 = (s32[320]{0:T(512)S(1)}, s32[320]{0:T(512)}, u32[]{:S(2)}) copy-start(s32[320]{0:T(512)} %copy-done.7) | copy-start | bytes 3844
  1145.4 2.6 copy-start.1
  1145.4 2.6 copy-start.6
  1148.0 17.8 %slice-start = ((s8[16777216]{0:T(1024)(128)(4,1)}), s8[4194304]{0:T(1024)(128)(4,1)S(1)}, s32[]{:S(2)}) async-start(s8[16777216]{0:T(1024)(128)(4,1)} %bitcast.83), calls=%async_computation.12 | async-start | bytes 8388608
  1149.8 16.0 %slice-start.1 = ((s8[16777216]{0:T(1024)(128)(4,1)}), s8[4194304]{0:T(1024)(128)(4,1)S(1)}, s32[]{:S(2)}) async-start(s8[16777216]{0:T(1024)(128)(4,1)} %bitcast.83), calls=%async_computation.13 | async-start | bytes 8388608
  1149.8 16.0 %slice-start.2 = ((s8[16777216]{0:T(1024)(128)(4,1)}), s8[4194304]{0:T(1024)(128)(4,1)S(1)}, s32[]{:S(2)}) async-start(s8[16777216]{0:T(1024)(128)(4,1)} %bitcast.83), calls=%async_computation.14 | async-start | bytes 8388608
  1149.8 16.0 %slice-start.3 = ((s8[16777216]{0:T(1024)(128)(4,1)}), s8[4194304]{0:T(1024)(128)(4,1)S(1)}, s32[]{:S(2)}) async-start(s8[16777216]{0:T(1024)(128)(4,1)} %bitcast.83), calls=%async_computation.15 | async-start | bytes 8388608
Sparse Core Ops, SparseCore 0:
  35.3 58.0 all-gather.10
  215.2 29.1 all-gather.8
  430.9 28.5 all-gather.6
  626.9 29.0 all-gather.4
  1031.2 55.0 reduce-scatter.1
where the time goes:
time: 1180 us
  waiting for transfers between devices  472 us (40%)
  blocking collectives  379 us (32%)
  local copies, waits for them, and re-layouts  207 us (18%)
  matrix products  47.8 us (4%)
  other arithmetic  31.4 us (3%)
  starting transfers between devices  27.8 us (2%)
  between operations  14 us (1%)
    all_to_all x1, blocking collectives, body(): lax.all_to_all(gate_cast, 'fs', split_axis=0, concat_axis=1, tiled=True)  188 us
    all_to_all x1, blocking collectives, body(): lax.all_to_all(up_cast, 'fs', split_axis=0, concat_axis=1, tiled=True)  186 us
    all_to_all x1, waiting for transfers between devices, body(): lax.all_to_all(down_cast, 'fs', split_axis=0, concat_axis=1, tiled=True)  172 us
    all_to_all x1, waiting for transfers between devices, body(): lax.all_to_all(down_rows, 'tp', split_axis=1, concat_axis=2, tiled=True)  150 us
    all_to_all x4, local copies, waits for them, and re-layouts, body(): lax.all_to_all(down_rows, 'tp', split_axis=1, concat_axis=2, tiled=True)  112 us
    all_to_all x1, waiting for transfers between devices, body(): lax.all_to_all(full_rows, 'fs', split_axis=0, concat_axis=0, tiled=True)  63.6 us
    reduce_scatter x1, waiting for transfers between devices, body(): lax.psum_scatter(partial_value.astype(jnp.bfloat16), 'tp', scatter_dimens...  55.2 us
    all_to_all x1, waiting for transfers between devices, body(): lax.all_to_all(summed, 'fs', split_axis=0, concat_axis=0, tiled=True)  31.2 us
  transfers between devices with their start and end apart: 9, of which 5 were waited for; matrix products, arithmetic and copies ran while one was open for 11% of the time, Pallas kernels for 0%

commit v1 on v0

v1 whole, which is shorter than its diff:
```python
import functools

import jax
import jax.numpy as jnp
from jax import lax
from jax.experimental import pallas as pl
from jax.experimental.pallas import tpu as pltpu
from jax.sharding import PartitionSpec as P

CAP = 30
SLOT = -(-CAP // 16) * 16
MESH = pl.DeviceIdType.MESH


def remote(src, dst, send, recv, device):
    copy = pltpu.make_async_remote_copy(
        src_ref=src, dst_ref=dst, send_sem=send, recv_sem=recv, device_id=device, device_id_type=MESH
    )
    copy.start()


def settle(ref, sem):
    pltpu.make_async_copy(ref, ref, sem).wait()


def loop(low, high, step):
    lax.fori_loop(low, high, lambda index, carry: (step(index), carry)[1], 0)


def span(index, size):
    return pl.ds(pl.multiple_of(index * size, size), size)


def greet(barrier, device):
    pl.semaphore_signal(barrier, inc=1, device_id=device, device_id_type=MESH)


def spread_kernel(
    sizes, tok, gate, up, down, arr, gate_out, up_out, down_out,
    own_tok, own, tok_send, tok_recv, share_send, share_recv,
    w_send, w_recv, twin_send, twin_recv, own_sem,
):
    n_gr, n_fs, n_tp = sizes
    gr, fs, tp = lax.axis_index("gr"), lax.axis_index("fs"), lax.axis_index("tp")
    per, blk, wide = gate_out.shape[0], gate.shape[1], gate.shape[2]
    per_tp = n_gr * n_fs // n_tp
    row = gr * n_fs + fs
    owner = row // per_tp
    home = tp * per_tp // n_fs
    ring = n_fs * n_tp

    barrier = pltpu.get_barrier_semaphore()

    def greet_plane(k):
        other = (fs * n_tp + tp + k) % ring
        greet(barrier, (gr, other // n_tp, other % n_tp))

    loop(1, ring, greet_plane)
    loop(1, n_gr, lambda k: greet(barrier, ((gr + k) % n_gr, fs, tp)))
    pl.semaphore_wait(barrier, ring + n_gr - 2)

    def tok_place(source, t):
        return arr.at[:, source, :, span(t, wide)]

    def rows_of(out, index):
        return out.at[:, span(index, blk), :]

    def down_place(index):
        return down_out.at[:, span(index, blk), span(tp, wide)]

    def mine(ref, f):
        return ref.at[pl.ds(f * per, per)]

    loads = [pltpu.make_async_copy(tok.at[fs], own_tok, own_sem.at[3])]
    for w, ref in enumerate((gate, up, down)):
        loads.append(pltpu.make_async_copy(mine(ref, fs), own.at[w], own_sem.at[w]))
    for load in loads:
        load.start()

    def far(k):
        return (fs + (k + n_fs // 2 - 1) % (n_fs - 1) + 1) % n_fs

    def send_tok(k):
        f = far(k)
        remote(tok.at[f], tok_place(fs, tp), tok_send, tok_recv.at[fs], (gr, f, tp))

    loop(0, n_fs - 1, send_tok)

    def send_down(k):
        f = far(k)
        remote(mine(down, f), down_place(row - owner * per_tp), w_send.at[2], w_recv.at[2, fs], (gr, f, owner))

    loop(0, n_fs - 1, send_down)
    for w, (ref, out) in enumerate(((gate, gate_out), (up, up_out))):

        def send_w(k, w=w, ref=ref, out=out):
            f = far(k)
            remote(mine(ref, f), rows_of(out, row), w_send.at[w], w_recv.at[w, fs], (gr, f, tp))

        loop(0, n_fs - 1, send_w)

    for load in loads:
        load.wait()
    pltpu.make_async_copy(own_tok, tok_place(fs, tp), tok_recv.at[fs]).start()
    pltpu.make_async_copy(own.at[0], rows_of(gate_out, row), w_recv.at[0, fs]).start()
    pltpu.make_async_copy(own.at[1], rows_of(up_out, row), w_recv.at[1, fs]).start()

    @pl.when(owner == tp)
    def _():
        pltpu.make_async_copy(own.at[2], down_place(row - owner * per_tp), w_recv.at[2, fs]).start()

    @pl.when(owner != tp)
    def _():
        remote(own.at[2], down_place(row - owner * per_tp), w_send.at[2], w_recv.at[2, fs], (gr, fs, owner))

    def share_tok(k):
        source = (fs + n_fs - k) % n_fs
        place = tok_place(source, tp)
        settle(place, tok_recv.at[source])
        for j in range(1, n_tp):
            t = (tp + j) % n_tp
            remote(place, place, share_send.at[t], share_recv.at[tp], (gr, fs, t))

    loop(0, n_fs, share_tok)

    @pl.when(home == gr)
    def _():
        def twin_down(k):
            source = tp * per_tp - gr * n_fs + k
            place = rows_of(down_out, k)
            settle(place, w_recv.at[2, source])
            for j in range(1, n_gr):
                g = (gr + j) % n_gr
                remote(place, place, twin_send.at[2, g], twin_recv.at[2, gr], (g, fs, tp))

        loop(0, per_tp, twin_down)

    for w, out in enumerate((gate_out, up_out)):

        def twin_w(k, w=w, out=out):
            source = (fs + n_fs - k) % n_fs
            place = rows_of(out, gr * n_fs + source)
            settle(place, w_recv.at[w, source])
            for j in range(1, n_gr):
                g = (gr + j) % n_gr
                remote(place, place, twin_send.at[w, g], twin_recv.at[w, gr], (g, fs, tp))

        loop(0, n_fs, twin_w)

    settle(tok.at[pl.ds(0, n_fs - 1)], tok_send)
    for w, ref in enumerate((gate, up)):
        settle(ref.at[pl.ds(0, (n_fs - 1) * per)], w_send.at[w])

    @pl.when(owner == tp)
    def _():
        settle(down.at[pl.ds(0, (n_fs - 1) * per)], w_send.at[2])

    @pl.when(owner != tp)
    def _():
        settle(down, w_send.at[2])

    for j in range(1, n_tp):
        t = (tp + j) % n_tp
        settle(arr.at[:, :, :, span(tp, wide)], share_send.at[t])
        settle(arr.at[:, :, :, span(t, wide)], share_recv.at[t])
    for j in range(1, n_gr):
        g = (gr + j) % n_gr
        for w, out in enumerate((gate_out, up_out)):
            settle(out.at[:, span(gr, n_fs * blk), :], twin_send.at[w, g])
            settle(out.at[:, span(g, n_fs * blk), :], twin_recv.at[w, g])

        @pl.when(home == gr)
        def _():
            settle(down_out, twin_send.at[2, g])

    @pl.when(home != gr)
    def _():
        settle(down_out, twin_recv.at[2, home])


def return_kernel(sizes, part, ret, got, summed, x_send, x_recv, z_send, z_recv):
    n_gr, n_fs, n_tp = sizes
    gr, fs, tp = lax.axis_index("gr"), lax.axis_index("fs"), lax.axis_index("tp")
    per, wide = part.shape[0], ret.shape[3]

    barrier = pltpu.get_barrier_semaphore()
    loop(1, n_fs, lambda k: greet(barrier, (gr, (fs + k) % n_fs, tp)))
    loop(1, n_tp, lambda k: greet(barrier, (gr, fs, (tp + k) % n_tp)))
    pl.semaphore_wait(barrier, n_fs + n_tp - 2)

    def exchange(x):
        for j in range(1, n_tp):
            t = (tp + j) % n_tp
            remote(part.at[x, :, :, span(t, wide)], got.at[tp, x], x_send.at[t], x_recv.at[tp, x], (gr, fs, t))

    loop(0, per, exchange)

    def reduce_one(x):
        for j in range(1, n_tp):
            t = (tp + j) % n_tp
            settle(got.at[t, x], x_recv.at[t, x])

        def add(f):
            total = part[x, f, :, span(tp, wide)].astype(jnp.float32)
            for j in range(1, n_tp):
                total = total + got[(tp + j) % n_tp, x, f].astype(jnp.float32)
            summed[x, f] = total.astype(jnp.bfloat16)

        loop(0, n_fs, add)
        ret[fs, x] = summed[x, fs]

        def send(k):
            f = (fs + (k + n_fs // 2 - 1) % (n_fs - 1) + 1) % n_fs
            remote(summed.at[x, f], ret.at[fs, x], z_send, z_recv.at[fs], (gr, f, tp))

        loop(0, n_fs - 1, send)

    loop(0, per, reduce_one)
    loop(1, n_fs, lambda k: settle(ret.at[(fs + k) % n_fs], z_recv.at[(fs + k) % n_fs]))
    settle(summed.at[:, pl.ds(0, n_fs - 1)], z_send)
    for j in range(1, n_tp):
        t = (tp + j) % n_tp
        settle(part.at[:, :, :, span(t, wide)], x_send.at[t])


def body(sizes, prompt, norm_gain, gate_weight, up_weight, down_weight, routes, route_weight):
    n_gr, n_fs, n_tp = sizes
    gate_cast = (gate_weight * norm_gain[None, :, None]).astype(jnp.bfloat16)
    up_cast = (up_weight * norm_gain[None, :, None]).astype(jnp.bfloat16)
    down_cast = down_weight.astype(jnp.bfloat16)
    values = prompt.astype(jnp.float32)
    tok_count, wide = prompt.shape
    full_width = wide * n_tp
    squares = jnp.sum(values * values, axis=-1, keepdims=True)
    total_squares = lax.psum(squares, "tp")
    normed = (values * lax.rsqrt(total_squares / full_width + 1e-06)).astype(jnp.bfloat16)
    experts, blk, _ = gate_weight.shape
    per = experts // n_fs
    slots_all = experts * SLOT
    picks_flat = routes.reshape(-1)
    matches = picks_flat[:, None] == jnp.arange(experts, dtype=jnp.int32)[None, :]
    order = jnp.arange(2 * tok_count, dtype=jnp.int32)
    before = (order[None, :] < order[:, None]).astype(jnp.bfloat16)
    earlier = jnp.dot(before, matches.astype(jnp.bfloat16), preferred_element_type=jnp.float32)
    slot_of = jnp.sum(jnp.where(matches, earlier, 0.0), axis=1).astype(jnp.int32)
    target = (picks_flat * SLOT + slot_of).reshape(tok_count, 2)
    slot_ids = jnp.arange(slots_all, dtype=jnp.int32)[None, :]
    select_first = (target[:, 0:1] == slot_ids).astype(jnp.bfloat16)
    select_second = (target[:, 1:2] == slot_ids).astype(jnp.bfloat16)
    select_both = select_first + select_second
    outbound = jnp.einsum("ts,td->sd", select_both, normed, preferred_element_type=jnp.float32)
    outbound = outbound.astype(jnp.bfloat16).reshape(n_fs, per, SLOT, wide)

    any_spec = pl.BlockSpec(memory_space=pl.ANY)
    rows = n_gr * n_fs * blk
    bf16 = jnp.bfloat16
    dma = pltpu.SemaphoreType.DMA
    arrived, gate_new, up_new, down_new = pl.pallas_call(
        functools.partial(spread_kernel, sizes),
        out_shape=(
            jax.ShapeDtypeStruct((per, n_fs, SLOT, full_width), bf16),
            jax.ShapeDtypeStruct((per, rows, wide), bf16),
            jax.ShapeDtypeStruct((per, rows, wide), bf16),
            jax.ShapeDtypeStruct((per, rows // n_tp, full_width), bf16),
        ),
        in_specs=[any_spec] * 4,
        out_specs=(any_spec,) * 4,
        scratch_shapes=[
            pltpu.VMEM((per, SLOT, wide), bf16),
            pltpu.VMEM((3, per, blk, wide), bf16),
            dma(()),
            dma((n_fs,)),
            dma((n_tp,)),
            dma((n_tp,)),
            dma((3,)),
            dma((3, n_fs)),
            dma((3, n_gr)),
            dma((3, n_gr)),
            dma((4,)),
        ],
        compiler_params=pltpu.CompilerParams(collective_id=0, has_side_effects=True),
        name="spread",
    )(outbound, gate_cast, up_cast, down_cast)

    arrived = arrived.reshape(per, n_fs * SLOT, full_width)
    gate_pre = jnp.einsum("xcd,xdh->xch", arrived, gate_new, preferred_element_type=jnp.float32)
    up_pre = jnp.einsum("xcd,xdh->xch", arrived, up_new, preferred_element_type=jnp.float32)
    hidden = (jax.nn.silu(gate_pre) * up_pre).astype(bf16)
    partial_value = jnp.einsum("xch,xhd->xcd", hidden, down_new, preferred_element_type=jnp.float32)
    partial_value = partial_value.astype(bf16).reshape(per, n_fs, SLOT, full_width)

    vmem_spec = pl.BlockSpec(memory_space=pltpu.VMEM)
    returned = pl.pallas_call(
        functools.partial(return_kernel, sizes),
        out_shape=jax.ShapeDtypeStruct((n_fs, per, SLOT, wide), bf16),
        in_specs=[vmem_spec],
        out_specs=vmem_spec,
        scratch_shapes=[
            pltpu.VMEM((n_tp, per, n_fs, SLOT, wide), bf16),
            pltpu.VMEM((per, n_fs, SLOT, wide), bf16),
            dma((n_tp,)),
            dma((n_tp, per)),
            dma(()),
            dma((n_fs,)),
        ],
        compiler_params=pltpu.CompilerParams(collective_id=1, has_side_effects=True),
        name="give_back",
    )(partial_value)
    returned_flat = returned.reshape(slots_all, wide)
    pick_first = jnp.dot(select_first, returned_flat, preferred_element_type=jnp.float32)
    pick_second = jnp.dot(select_second, returned_flat, preferred_element_type=jnp.float32)
    mixed = route_weight[:, 0:1] * pick_first + route_weight[:, 1:2] * pick_second
    return (gate_new, up_new, down_new, mixed.astype(bf16))


def solution(mesh):
    sizes = (mesh.shape["gr"], mesh.shape["fs"], mesh.shape["tp"])
    return jax.shard_map(
        functools.partial(body, sizes),
        mesh=mesh,
        in_specs=(
            P(("gr", "fs"), "tp"),
            P(("gr", "fs")),
            P(None, ("gr", "fs"), "tp"),
            P(None, ("gr", "fs"), "tp"),
            P(None, ("gr", "fs"), "tp"),
            P(("gr", "fs"), None),
            P(("gr", "fs"), None),
        ),
        out_specs=(
            P("fs", None, "tp"),
            P("fs", None, "tp"),
            P("fs", "tp", None),
            P(("gr", "fs"), "tp"),
        ),
        check_vma=False,
    )
```

time: 1180 us -> 780 us (0.66)
  Pallas kernels: 0 us -> 669 us
  waiting for transfers between devices: 472 us -> 0 us
  blocking collectives: 379 us -> 5.87 us
  local copies, waits for them, and re-layouts: 207 us -> 37.4 us
  starting transfers between devices: 27.8 us -> 0 us
  between operations: 14 us -> 0.81 us
    pallas_call x0 -> x2, Pallas kernels: none -> 669 us  [the longest x1 603 us: body(): pl.pallas_call(functools.partial(spread_kernel, sizes), out_shape=(jax.Sh...]
    all_to_all x4 -> x0, waiting for transfers between devices: 417 us -> none  [the longest x1 172 us: body(): lax.all_to_all(down_cast, 'fs', split_axis=0, concat_axis=1, tiled=True)]
    all_to_all x2 -> x0, blocking collectives: 374 us -> none  [the longest x1 188 us: body(): lax.all_to_all(gate_cast, 'fs', split_axis=0, concat_axis=1, tiled=True)]
    all_to_all x8 -> x0, local copies, waits for them, and re-layouts: 139 us -> none  [the longest x4 112 us: body(): lax.all_to_all(down_rows, 'tp', split_axis=1, concat_axis=2, tiled=True)]
    reduce_scatter x1 -> x0, waiting for transfers between devices: 55.2 us -> none  [body(): lax.psum_scatter(partial_value.astype(jnp.bfloat16), 'tp', scatter_dimens...]
    all_gather x2 -> x0, local copies, waits for them, and re-layouts: 30 us -> none  [the longest x1 22.3 us: body(): lax.all_gather(spread[2], 'gr', axis=1, tiled=True)]
    all_to_all x4 -> x0, starting transfers between devices: 27.6 us -> none  [the longest x1 9.67 us: body(): lax.all_to_all(down_rows, 'tp', split_axis=1, concat_axis=2, tiled=True)]
    unnamed x31 -> x34, local copies, waits for them, and re-layouts: 29.6 us -> 37 us
  transfers between devices with their start and end apart: 9 -> 0, of which waited for: 5 -> 0; matrix products, arithmetic and copies ran while one was open for 11% -> 0% of each run, Pallas kernels for 0% -> 0%
where the time goes in v1:
time: 780 us; the launch traced here: 779 us
  Pallas kernels  669 us (86%)
  matrix products  41.6 us (5%)
  local copies, waits for them, and re-layouts  37.4 us (5%)
  other arithmetic  24.2 us (3%)
    pallas_call x1, Pallas kernels, body(): pl.pallas_call(functools.partial(spread_kernel, sizes), out_shape=(jax.Sh...  603 us
    pallas_call x1, Pallas kernels, body(): pl.pallas_call(functools.partial(return_kernel, sizes), out_shape=jax.Sha...  66.1 us
    unnamed x34, local copies, waits for them, and re-layouts  37 us
    dot_general x1, matrix products, body(): jnp.einsum('xch,xhd->xcd', hidden, down_new, preferred_element_type=jnp.f...  19.5 us
    convert_element_type x1, other arithmetic, body(): up_cast = (up_weight * norm_gain[None, :, None]).astype(jnp.bfloat16)  18.2 us

profile of v1, /device:TPU:0, one launch (start us, length us, event | category | flops | bytes accessed | tf_op | source)
XLA Modules:
  0.0 779.4 jit_solution(11627898848858841760)
XLA Ops:
  0.6 0.8 copy.17
  1.5 0.1 eq.45
  1.6 0.3 fusion.11
  1.9 0.1 convert_element_type.43
  2.1 0.1 copy.18
  2.2 0.7 multiply_add_fusion
  2.9 1.3 fusion.6
  4.2 5.9 psum.7
  10.1 3.9 convolution_convert_fusion.1
  14.0 0.0 slice-start.3
  14.0 18.2 %multiply_convert_fusion = (bf16[32,128,1024]{2,1,0:T(8,128)(2,1)}, bf16[32,128,1024]{2,1,0:T(8,128)(2,1)}) fusion(f32[32,128,1024]{2,1,0:T(8,128)} %param.10, f32[128]{0:T(128)S(1)} %copy-done.2, f32[32,128,1024]{2,1,0:T(8,128)} %param.9), kind=kLoop, calls=%fused_computation | loop fusion | flops 16777216 | bytes 50332160 | tf_op jit(solution)/shard_map/convert_element_type | solution.py:229
  32.2 0.9 slice-done.1
  33.1 1.3 slice-done.2
  34.4 1.2 slice-done.3
  35.6 4.0 convert_element_type.51.down
  39.6 603.3 %spread.1 = (bf16[4,8,32,2048]{3,2,1,0:T(8,128)(2,1)}, bf16[4,2048,1024]{2,1,0:T(8,128)(2,1)}, bf16[4,2048,1024]{2,1,0:T(8,128)(2,1)}, bf16[4,1024,2048]{2,1,0:T(8,128)(2,1)}) custom-call(bf16[8,4,32,1024]{3,2,1,0:T(8,128)(2,1)} %bitcast.20, bf16[32,128,1024]{2,1,0:T(8,128)(2,1)} %get-tuple-element.17.gate, bf16[32,128,1024]{2,1,0:T(8,128)(2,1)} %get-tuple-element.16.up, ...), custom_call_target="tpu_custom_call" | custom-call | tf_op jit(solution)/shard_map/spread/pallas_call | solution.py:258
  642.9 13.6 %fusion.23 = f32[4,256,1024]{2,1,0:T(8,128)} fusion(bf16[4,256,2048]{2,1,0:T(8,128)(2,1)} %bitcast.21, bf16[4,2048,1024]{2,1,0:T(8,128)(2,1)} %get-tuple-element.22), kind=kOutput, calls=%fused_computation.38 | convolution fusion | flops 4294967296 | bytes 25165824 | tf_op jit(solution)/shard_map/xcd,xdh->xch/dot_general | solution.py:286
  656.5 19.5 %convolution_convert_fusion = bf16[4,256,2048]{2,1,0:T(8,128)(2,1)} fusion(bf16[4,1024,2048]{2,1,0:T(8,128)(2,1)} %get-tuple-element.24, f32[4,256,1024]{2,1,0:T(8,128)} %fusion.23, bf16[4,256,2048]{2,1,0:T(8,128)(2,1)} %bitcast.22, bf16[4,2048,1024]{2,1,0:T(8,128)(2,1)} %get-tuple-element.23), kind=kOutput, calls=%fused_computation.3 | convolution fusion | flops 8598323200 | bytes 46137344 | tf_op jit(solution)/shard_map/xch,xhd->xcd/dot_general | solution.py:289
  675.9 66.1 %give_back.1 = bf16[8,4,32,1024]{3,2,1,0:T(8,128)(2,1)} custom-call(bf16[4,8,32,2048]{3,2,1,0:T(8,128)(2,1)} %bitcast.17), custom_call_target="tpu_custom_call" | custom-call | tf_op jit(solution)/shard_map/give_back/pallas_call | solution.py:293
  742.1 2.6 convolution_multiply_fusion.1
  744.8 0.0 copy-done
  744.8 0.0 slice-start.8
  744.8 1.8 fusion.5
  746.6 0.0 slice-start.5
  746.6 16.7 %copy.22 = bf16[4,2048,1024]{2,1,0:T(8,128)(2,1)} copy(bf16[4,2048,1024]{2,1,0:T(8,128)(2,1)} %get-tuple-element.22) | data formatting | bytes 33554432
  763.2 0.0 slice-done.9
  763.3 0.0 slice-start.6
  763.3 0.0 slice-start.7
  763.3 8.5 %copy.23 = bf16[4,2048,1024]{2,1,0:T(8,128)(2,1)} copy(bf16[4,2048,1024]{2,1,0:T(8,128)(2,1)S(1)} %bitcast.16) | data formatting | bytes 33554432
  771.8 0.0 slice-done.5
  771.8 1.4 slice-done.7
  773.2 6.2 copy.24
  (26 shorter events, 0.1 us)
Async XLA Ops:
  0.6 13.4 %copy-start.2 = (f32[128]{0:T(128)S(1)}, f32[128]{0:T(128)}, u32[]{:S(2)}) copy-start(f32[128]{0:T(128)} %param.8) | copy-start | bytes 1540
  14.0 18.2 %slice-start = ((s8[16777216]{0:T(1024)(128)(4,1)}), s8[4194304]{0:T(1024)(128)(4,1)S(1)}, s32[]{:S(2)}) async-start(s8[16777216]{0:T(1024)(128)(4,1)} %bitcast.11), calls=%async_computation | async-start | bytes 8388608
  14.0 19.1 %slice-start.1 = ((s8[16777216]{0:T(1024)(128)(4,1)}), s8[4194304]{0:T(1024)(128)(4,1)S(1)}, s32[]{:S(2)}) async-start(s8[16777216]{0:T(1024)(128)(4,1)} %bitcast.11), calls=%async_computation.1 | async-start | bytes 8388608
  14.0 20.3 %slice-start.2 = ((s8[16777216]{0:T(1024)(128)(4,1)}), s8[4194304]{0:T(1024)(128)(4,1)S(1)}, s32[]{:S(2)}) async-start(s8[16777216]{0:T(1024)(128)(4,1)} %bitcast.11), calls=%async_computation.2 | async-start | bytes 8388608
  14.0 21.5 %slice-start.3 = ((s8[16777216]{0:T(1024)(128)(4,1)}), s8[4194304]{0:T(1024)(128)(4,1)S(1)}, s32[]{:S(2)}) async-start(s8[16777216]{0:T(1024)(128)(4,1)} %bitcast.11), calls=%async_computation.3 | async-start | bytes 8388608
  675.9 66.2 %copy-start.1 = (f32[320,2]{0,1:T(2,128)S(1)}, f32[320,2]{0,1:T(2,128)}, u32[]{:S(2)}) copy-start(f32[320,2]{0,1:T(2,128)} %param.13) | copy-start | bytes 7684
  742.1 2.7 copy-start
  744.8 18.5 %slice-start.8 = ((s8[16777216]{0:T(1024)(128)(4,1)}), s8[4194304]{0:T(1024)(128)(4,1)S(1)}, s32[]{:S(2)}) async-start(s8[16777216]{0:T(1024)(128)(4,1)} %bitcast.15), calls=%async_computation.8 | async-start | bytes 8388608
  746.6 16.7 %slice-start.9 = ((s8[16777216]{0:T(1024)(128)(4,1)}), s8[4194304]{0:T(1024)(128)(4,1)S(1)}, s32[]{:S(2)}) async-start(s8[16777216]{0:T(1024)(128)(4,1)} %bitcast.15), calls=%async_computation.9 | async-start | bytes 8388608
  746.6 16.7 %slice-start.10 = ((s8[16777216]{0:T(1024)(128)(4,1)}), s8[4194304]{0:T(1024)(128)(4,1)S(1)}, s32[]{:S(2)}) async-start(s8[16777216]{0:T(1024)(128)(4,1)} %bitcast.15), calls=%async_computation.10 | async-start | bytes 8388608
  746.6 16.7 %slice-start.11 = ((s8[16777216]{0:T(1024)(128)(4,1)}), s8[4194304]{0:T(1024)(128)(4,1)S(1)}, s32[]{:S(2)}) async-start(s8[16777216]{0:T(1024)(128)(4,1)} %bitcast.15), calls=%async_computation.11 | async-start | bytes 8388608
  746.6 25.2 %slice-start.4 = ((s8[16777216]{0:T(1024)(128)(4,1)}), s8[4194304]{0:T(1024)(128)(4,1)S(1)}, s32[]{:S(2)}) async-start(s8[16777216]{0:T(1024)(128)(4,1)} %bitcast.13), calls=%async_computation.4 | async-start | bytes 8388608
  746.6 25.2 %slice-start.5 = ((s8[16777216]{0:T(1024)(128)(4,1)}), s8[4194304]{0:T(1024)(128)(4,1)S(1)}, s32[]{:S(2)}) async-start(s8[16777216]{0:T(1024)(128)(4,1)} %bitcast.13), calls=%async_computation.5 | async-start | bytes 8388608
  763.3 8.5 %slice-start.6 = ((s8[16777216]{0:T(1024)(128)(4,1)}), s8[4194304]{0:T(1024)(128)(4,1)S(1)}, s32[]{:S(2)}) async-start(s8[16777216]{0:T(1024)(128)(4,1)} %bitcast.13), calls=%async_computation.6 | async-start | bytes 8388608
  763.3 10.0 %slice-start.7 = ((s8[16777216]{0:T(1024)(128)(4,1)}), s8[4194304]{0:T(1024)(128)(4,1)S(1)}, s32[]{:S(2)}) async-start(s8[16777216]{0:T(1024)(128)(4,1)} %bitcast.13), calls=%async_computation.7 | async-start | bytes 8388608
